TPU v7x, 256 devices: a whole 4x4x8 slice. The times are simulated.
256 devices in a mesh: sp: 32 (over z, x), tp: 8 (over y, core).
Axes of the slice: x: 4, y: 4, z: 8, core: 2. Of those that a mesh axis runs over, the one named last changes fastest.
Arguments:
- tokens: bfloat16 [24576, 2048], P(('sp', 'tp')), may hold values from -6 to 6
- in_gain: float32 [2048], replicated, may hold values from 0.1 to 1.9
- w_query: bfloat16 [2048, 1024], P(None, 'tp'), may hold values from -0.125 to 0.125
- w_key: bfloat16 [2048, 1024], P(None, 'tp'), may hold values from -0.125 to 0.125
- w_value: bfloat16 [2048, 2048], P(None, 'tp'), may hold values from -0.125 to 0.125
- w_input_gate: bfloat16 [2048, 8], replicated, may hold values from -8 to 8
- w_forget_gate: bfloat16 [2048, 8], replicated, may hold values from -0.125 to 0.125
- forget_bias: float32 [8], replicated
- forget_extra: float32 [24576, 8], P('sp', 'tp'), may hold values from -2 to 0
- w_conv_gate: bfloat16 [2048, 2048], P(None, 'tp'), may hold values from -0.125 to 0.125
- w_conv_left: bfloat16 [2048, 2048], P(None, 'tp'), may hold values from -0.125 to 0.125
- w_conv_right: bfloat16 [2048, 2048], P(None, 'tp'), may hold values from -0.125 to 0.125
- conv_taps: float32 [3, 2048], replicated, may hold values from -3.5 to 3.5
- first_memory: float32 [8, 128, 256], P('tp'), may hold values from -5120 to 5120
- first_norm: float32 [8, 128], P('tp'), may hold values from -5120 to 5120
- w_out_memory: bfloat16 [2048, 2048], P('tp'), may hold values from -0.09375 to 0.09375
- w_out_conv: bfloat16 [2048, 2048], P('tp'), may hold values from -0.09375 to 0.09375
Outputs:
- mixed: bfloat16 [24576, 2048], P(('sp', 'tp'))
All inputs are finite; a program needn't handle non-finite values.
Results may differ from a plain program's by a relative error of at most 0.015.
The roundings to bfloat16 on the way count: a program that leaves them out, or rounds other values in their place, can miss the bound.
Values may be sent and summed in bfloat16 or wider, within the bound.
A program may use at most 64 MiB of HBM per device.

v0:
```python
import jax
import jax.numpy as jnp
from jax import lax
from jax.sharding import Mesh
from jax.sharding import PartitionSpec as P

KEY_DIM = 128
VALUE_DIM = 256
TAPS = 3
V_WIDTH = 2048
SP = ("sp_0", "sp_1")
SP_TP = ("sp_0", "sp_1", "tp")
epsilon = 1e-06
very_negative = -1e30
highest = lax.Precision.HIGHEST


def from_behind(block, axis, distance):
    devices = range(lax.axis_size(axis))
    route = [(i - distance, i) for i in devices if i - distance in devices]
    return lax.ppermute(block, axis, route)


def filled_with(x, identity):
    return jax.tree.map(
        lambda part, zero: jnp.zeros_like(part) + jnp.asarray(zero, part.dtype), x, identity
    )


def collected_together(x, axis):
    leaves = jax.tree.leaves(x)
    sequence = sorted(range(len(leaves)), key=lambda k: -leaves[k].size)
    width = (1, *leaves[sequence[0]].shape)[-1]
    lines = [
        jnp.pad(leaves[k].reshape(-1), (0, -leaves[k].size % width)).reshape(-1, width)
        for k in sequence
    ]
    both, at, found = (lax.all_gather(jnp.concatenate(lines), axis), 0, {})
    for k, line in zip(sequence, lines):
        slab = both[:, at : at + len(line)].reshape(len(both), -1)
        found[k] = slab[:, : leaves[k].size].reshape(-1, *leaves[k].shape)
        at += len(line)
    numbers = iter(range(len(leaves)))
    return jax.tree.map(lambda _: found[next(numbers)], x)


def entering(x, axes, combine, identity):
    before = start = filled_with(x, identity)
    running = x
    for axis in reversed(axes):
        size, here = (lax.axis_size(axis), lax.axis_index(axis))
        pieces = collected_together(running, axis)
        inside, running = (start, start)
        for k in range(size):
            passed = k < here
            running = combine(running, jax.tree.map(lambda part: part[k], pieces))
            inside = jax.tree.map(lambda new, old: jnp.where(passed, new, old), running, inside)
        before = combine(inside, before)
    return before


def rounded(values):
    return lax.optimization_barrier(values.astype(jnp.bfloat16)).astype(jnp.float32)


def join_states(earlier, later):
    decay_early, max_early, memory_early, norm_early = earlier
    decay_late, max_late, memory_late, norm_late = later
    joined_max = jnp.maximum(max_early + decay_late, max_late)
    scale_early = jnp.exp(max_early + decay_late - joined_max)
    scale_late = jnp.exp(max_late - joined_max)
    joined_memory = (
        scale_early[:, None, None] * memory_early + scale_late[:, None, None] * memory_late
    )
    joined_norm = scale_early[:, None] * norm_early + scale_late[:, None] * norm_late
    return (decay_early + decay_late, joined_max, joined_memory, joined_norm)


def per_device(
    tokens,
    in_gain,
    w_query,
    w_key,
    w_value,
    w_input_gate,
    w_forget_gate,
    forget_bias,
    forget_extra,
    w_conv_gate,
    w_conv_left,
    w_conv_right,
    conv_taps,
    first_memory,
    first_norm,
    w_out_memory,
    w_out_conv,
):
    heads_here = w_query.shape[1] // KEY_DIM
    query_width = heads_here * KEY_DIM
    value_width = heads_here * VALUE_DIM
    channels = w_conv_gate.shape[1]
    head_first = lax.axis_index("tp") * heads_here
    channel_first = lax.axis_index("tp") * channels
    input_gate = lax.dynamic_slice_in_dim(w_input_gate, head_first, heads_here, 1)
    forget_gate = lax.dynamic_slice_in_dim(w_forget_gate, head_first, heads_here, 1)
    bias_here = lax.dynamic_slice_in_dim(forget_bias, head_first, heads_here, 0)
    taps_here = lax.dynamic_slice_in_dim(conv_taps, channel_first, channels, 1)
    token_rows = tokens.astype(jnp.float32)
    scale_rows = lax.rsqrt(jnp.mean(token_rows * token_rows, axis=1, keepdims=True) + epsilon)
    normed = (token_rows * scale_rows * in_gain).astype(jnp.bfloat16)
    sub_rows = lax.all_gather(normed, "tp", axis=0, tiled=True)
    pieces = [
        jnp.dot(sub_rows, weight, preferred_element_type=jnp.float32)
        for weight in (
            w_query,
            w_key,
            w_value,
            w_conv_gate,
            w_conv_left,
            w_conv_right,
            input_gate,
            forget_gate,
        )
    ]
    projected = jnp.concatenate(pieces, axis=1)
    row_count = projected.shape[0]
    offset_value = 2 * query_width
    offset_conv = offset_value + value_width
    offset_gate = offset_conv + 3 * channels
    query_rows = (
        projected[:, 0:query_width].astype(jnp.bfloat16).reshape(row_count, heads_here, KEY_DIM)
    )
    key_rows = (
        projected[:, query_width:offset_value]
        .astype(jnp.bfloat16)
        .reshape(row_count, heads_here, KEY_DIM)
    )
    value_rows = (
        projected[:, offset_value:offset_conv]
        .astype(jnp.bfloat16)
        .reshape(row_count, heads_here, VALUE_DIM)
    )
    conv_gate = rounded(projected[:, offset_conv : offset_conv + channels])
    conv_left = rounded(projected[:, offset_conv + channels : offset_conv + 2 * channels])
    conv_right = rounded(projected[:, offset_conv + 2 * channels : offset_gate])
    in_pre = projected[:, offset_gate : offset_gate + heads_here]
    forget_pre = projected[:, offset_gate + heads_here : offset_gate + 2 * heads_here] + bias_here
    log_forget = jax.nn.log_sigmoid(forget_pre) + forget_extra
    cumulative = jnp.cumsum(log_forget, axis=0)
    decay_total = cumulative[row_count - 1]
    weight_log = decay_total[None, :] - cumulative + in_pre
    block_max = jnp.max(weight_log, axis=0)
    keyed = key_rows.astype(jnp.float32) * jnp.exp(weight_log - block_max[None, :])[:, :, None]
    block_norm = jnp.sum(keyed, axis=0)
    block_memory = jnp.einsum(
        "shd,shv->hdv", keyed.astype(jnp.bfloat16), value_rows, preferred_element_type=jnp.float32
    )
    product = (conv_left * conv_right).astype(jnp.bfloat16)
    edge_rows = product[row_count - (TAPS - 1) :]
    before_rows = from_behind(edge_rows, SP, 1)
    prior_decay, prior_max, prior_memory, prior_norm = entering(
        (decay_total, block_max, block_memory, block_norm),
        SP,
        join_states,
        (
            jnp.zeros_like(decay_total),
            jnp.full_like(block_max, very_negative),
            jnp.zeros_like(block_memory),
            jnp.zeros_like(block_norm),
        ),
    )
    enter_max = jnp.maximum(prior_max, prior_decay)
    from_prior = jnp.exp(prior_max - enter_max)
    from_first = jnp.exp(prior_decay - enter_max)
    carry_memory = (
        from_prior[:, None, None] * prior_memory + from_first[:, None, None] * first_memory
    )
    carry_norm = from_prior[:, None] * prior_norm + from_first[:, None] * first_norm
    query_scale = KEY_DIM ** (-0.5)
    row_ids = lax.iota(jnp.int32, row_count)
    causal = row_ids[:, None] >= row_ids[None, :]
    cum_heads = cumulative.T
    log_gap = cum_heads[:, :, None] - cum_heads[:, None, :] + in_pre.T[:, None, :]
    log_gap = jnp.where(causal[None], log_gap, -jnp.inf)
    inter_log = cum_heads + enter_max[:, None]
    row_max = jnp.maximum(inter_log, jnp.max(log_gap, axis=2))
    raw_scores = (
        jnp.einsum("thd,shd->hts", query_rows, key_rows, preferred_element_type=jnp.float32)
        * query_scale
    )
    mixing = raw_scores * jnp.exp(log_gap - row_max[:, :, None])
    carried = jnp.exp(inter_log - row_max).T
    scaled_query = query_rows.astype(jnp.float32) * query_scale
    from_values = jnp.einsum(
        "hts,shv->thv", mixing.astype(jnp.bfloat16), value_rows, preferred_element_type=jnp.float32
    )
    from_memory = jnp.einsum("thd,hdv->thv", scaled_query, carry_memory, precision=highest)
    from_norm = jnp.einsum("thd,hd->th", scaled_query, carry_norm, precision=highest)
    numerator = from_values + carried[:, :, None] * from_memory
    denominator = jnp.sum(mixing, axis=2).T + carried * from_norm
    memory_out = numerator / jnp.maximum(jnp.abs(denominator), 1.0)[:, :, None]
    local_squares = jnp.sum(memory_out * memory_out, axis=(1, 2))
    row_total = lax.psum(local_squares, "tp")
    row_scale = lax.rsqrt(row_total / V_WIDTH + epsilon)
    heads_out = memory_out * row_scale[:, None, None]
    heads_out = heads_out.reshape(row_count, value_width).astype(jnp.bfloat16)
    padded = jnp.concatenate([before_rows, product], axis=0).astype(jnp.float32)
    filtered = taps_here[0][None, :] * padded[0:row_count]
    for tap_index in range(1, TAPS):
        filtered = (
            filtered + taps_here[tap_index][None, :] * padded[tap_index : tap_index + row_count]
        )
    conv_branch = (conv_gate * filtered).astype(jnp.bfloat16)
    return lax.psum_scatter(
        (
            jnp.dot(heads_out, w_out_memory, preferred_element_type=jnp.float32)
            + jnp.dot(conv_branch, w_out_conv, preferred_element_type=jnp.float32)
        ).astype(jnp.bfloat16),
        "tp",
        scatter_dimension=0,
        tiled=True,
    )


def solution(mesh):
    split = Mesh(mesh.devices.reshape(8, 4, mesh.shape["tp"]), ("sp_0", "sp_1", "tp"))
    placed = (
        P(SP_TP, None),
        P(),
        P(None, "tp"),
        P(None, "tp"),
        P(None, "tp"),
        P(),
        P(),
        P(),
        P(SP, "tp"),
        P(None, "tp"),
        P(None, "tp"),
        P(None, "tp"),
        P(),
        P("tp", None, None),
        P("tp", None),
        P("tp", None),
        P("tp", None),
    )
    return jax.shard_map(
        per_device, mesh=split, in_specs=placed, out_specs=P(SP_TP, None), check_vma=False
    )
```

profile of v0, /device:TPU:2, one launch (start us, length us, event | category | flops | bytes accessed | tf_op | source)
XLA Modules:
  0.0 207.4 jit_solution(9044216374947095805)
XLA Ops:
  6.5 1.3 fusion.4
  7.8 1.9 fusion.6
  9.8 1.2 dynamic_slice.13
  11.0 0.9 constant_dynamic-slice_fusion
  11.9 31.2 %all-gather.7.cloned.1.call-done = bf16[768,2048]{1,0:T(8,128)(2,1)} async-done(((bf16[96,2048]{1,0:T(8,128)(2,1)}), bf16[768,2048]{1,0:T(8,128)(2,1)}) %all-gather.7.cloned.1.call-update) | async-done | bytes 3145744 | tf_op jit(solution)/shard_map/all_gather | solution.py:111
  43.1 2.8 %convolution_reduce_fusion.1 = f32[768]{0:T(1024)S(1)} fusion(bf16[768,2048]{1,0:T(8,128)(2,1)} %all-gather.7.cloned.1.call-done, bf16[2048,8]{0,1:T(8,128)(2,1)} %param.23, s32[]{:T(128)S(6)} %select_n.346), kind=kOutput, calls=%fused_computation.18 | convolution fusion | flops 3145728 | bytes 3156996 | tf_op jit(solution)/shard_map/dot_general | solution.py:113
  46.0 0.6 fusion.118
  46.5 0.3 reduce-window.6
  46.8 0.2 slice_reduce_fusion
  47.0 0.2 reduce-window.9
  47.2 0.6 slice.336
  47.9 0.6 slice.337
  49.6 3.0 %convolution_reduce_fusion = f32[768]{0:T(1024)S(1)} fusion(bf16[768,2048]{1,0:T(8,128)(2,1)} %all-gather.7.cloned.1.call-done, bf16[2048,8]{0,1:T(8,128)(2,1)} %param.22, s32[]{:T(128)S(6)} %select_n.346), kind=kOutput, calls=%fused_computation.17 | convolution fusion | flops 3145728 | bytes 3156996 | tf_op jit(solution)/shard_map/dot_general | solution.py:113
  52.6 0.6 fusion.119
  53.3 0.5 pad.22
  53.8 0.5 subtract_exponential_fusion.1
  54.4 1.0 fusion.19
  55.4 0.2 copy-done.6
  55.6 1.0 convolution_convert_fusion.3
  56.6 0.4 fusion.21
  57.0 13.5 %all-gather.2 = f32[4,131,256]{2,1,0:T(8,128)S(1)} all-gather(f32[1,131,256]{2,1,0:T(8,128)S(1)} %maximum_bitcast_fusion), channel_id=2, replica_groups=mesh['sp_0'=8,'sp_1'=4,'tp'=8] {'sp_1'}, dimensions={0}, use_global_device_ids=true | all-gather | bytes 670720 | tf_op jit(solution)/shard_map/all_gather | solution.py:38
  70.6 0.6 fusion.192
  71.2 0.6 fusion.193
  82.5 0.7 maximum_bitcast_fusion.1
  83.3 3.3 %convolution_convert_fusion = bf16[768,256]{1,0:T(8,128)(2,1)S(1)} fusion(bf16[768,2048]{1,0:T(8,128)(2,1)} %all-gather.7.cloned.1.call-done, bf16[2048,256]{1,0:T(8,128)(2,1)} %param.28), kind=kOutput, calls=%fused_computation.10 | convolution fusion | flops 805502976 | bytes 4587520 | tf_op jit(solution)/shard_map/dot_general | solution.py:113
  86.6 0.1 copy-done.7
  86.7 1.0 convolution_convert_fusion.1
  87.7 0.1 multiply_convert_fusion
  87.8 2.1 collective-permute-start
  89.9 1.0 convolution_convert_fusion.5
  90.9 1.7 convolution_convert_fusion.2
  92.6 0.3 select_reduce_fusion
  93.7 0.1 maximum_convert_fusion
  93.8 27.6 %all-gather.9.cloned.1.call-done = f32[8,131,256]{2,1,0:T(8,128)} async-done(((f32[1,131,256]{2,1,0:T(8,128)}), f32[8,131,256]{2,1,0:T(8,128)}) %all-gather.9.cloned.1.call-update) | async-done | bytes 1073168 | tf_op jit(solution)/shard_map/all_gather | solution.py:38
  121.5 1.0 fusion.188
  122.4 0.6 fusion.190
  123.0 0.6 fusion.191
  144.8 0.7 fusion.194
  145.5 0.5 convolution_bitcast_fusion
  146.0 0.1 copy-done.12
  146.2 0.5 convolution_reduce_fusion.2
  146.6 2.5 %multiply_reduce_fusion = (f32[768]{0:T(1024)S(1)}, f32[1,256,768]{2,1,0:T(8,128)S(1)}) fusion(f32[768]{0:T(1024)S(1)} %get-tuple-element.5, f32[1,256,768]{2,1,0:T(8,128)S(1)} %convolution_bitcast_fusion, bf16[768,128]{1,0:T(8,128)(2,1)S(1)} %convolution_convert_fusion.5, f32[8,131,256]{2,1,0:T(8,128)} %all-gather.9.cloned.1.call-done, ...), kind=kOutput, calls=%fused_computation.34 | convolution fusion | flops 305200384 | bytes 3902464 | tf_op jit(solution)/shard_map/thd,hdv->thv/dot_general | solution.py:197
  149.1 12.4 %psum.7 = f32[768]{0:T(1024)S(1)} all-reduce(f32[768]{0:T(1024)S(1)} %get-tuple-element.48), channel_id=1, replica_groups=mesh['sp_0'=8,'sp_1'=4,'tp'=8] {'tp'}, use_global_device_ids=true, to_apply=%region_8.9 | all-reduce | flops 768 | bytes 6144 | tf_op jit(solution)/shard_map/psum | solution.py:203
  161.6 1.0 fusion.12
  162.6 0.2 copy-done.3
  162.8 0.1 copy-done.4
  162.9 2.9 %add_convert_fusion = bf16[768,2048]{1,0:T(8,128)(2,1)} fusion(f32[768,2048]{1,0:T(8,128)S(1)} %fusion.12, bf16[256,2048]{1,0:T(8,128)(2,1)S(1)} %copy-done.3, f32[770,256]{1,0:T(8,128)S(1)} %maximum_convert_fusion, bf16[768,256]{1,0:T(8,128)(2,1)S(1)} %copy-done.4, f32[256]{0:T(256)S(1)} %bitcast.178, f32[256]{0:T(256)S(1)} %bitcast.177, f32[256]{0:T(256)S(1)} %bitcast.176), kind=kOutput, calls=%fused_computation | convolution fusion | flops 810024960 | bytes 13241344 | tf_op jit(solution)/shard_map/dot_general | solution.py:217
  165.8 35.1 %reduce-scatter.2.cloned.1.call-done = bf16[96,2048]{1,0:T(8,128)(2,1)} async-done(((bf16[768,2048]{1,0:T(8,128)(2,1)}), bf16[96,2048]{1,0:T(8,128)(2,1)}) %reduce-scatter.2.cloned.1.call-update) | async-done | bytes 393232 | tf_op jit(solution)/shard_map/reduce_scatter | solution.py:214
  (52 shorter events, 0.5 us)
Async XLA Ops:
  6.5 155.0 %copy-start = (bf16[256,2048]{1,0:T(8,128)(2,1)S(1)}, bf16[256,2048]{1,0:T(8,128)(2,1)}, u32[]{:S(2)}) copy-start(bf16[256,2048]{1,0:T(8,128)(2,1)} %param.32) | copy-start | bytes 3145732
  6.5 36.6 %all-gather.7.cloned.1.call-start = ((), (), s32[]{:S(2)}) async-start(), calls=%async_computation.1 | async-start | bytes 3538944 | tf_op jit(solution)/shard_map/all_gather | solution.py:111
  9.8 111.7 %all-gather.9.cloned.1.call-start = ((), (), s32[]{:S(2)}) async-start(), calls=%async_computation.3 | async-start | bytes 1253376 | tf_op jit(solution)/shard_map/all_gather | solution.py:38
  11.9 34.6 %copy-start.5 = (f32[768,1]{0,1:T(1,128)S(1)}, f32[768,1]{0,1:T(1,128)}, u32[]{:S(2)}) copy-start(f32[768,1]{0,1:T(1,128)} %param.25) | copy-start | bytes 9220
  49.6 4.8 %copy-start.1 = (bf16[768,2048]{1,0:T(8,128)(2,1)S(1)}, bf16[768,2048]{1,0:T(8,128)(2,1)}, u32[]{:S(2)}) copy-start(bf16[768,2048]{1,0:T(8,128)(2,1)} %all-gather.7.cloned.1.call-done) | copy-start | bytes 9437188
  49.6 4.8 %copy-start.9 = (bf16[2048,128]{1,0:T(8,128)(2,1)S(1)}, bf16[2048,128]{1,0:T(8,128)(2,1)}, u32[]{:S(2)}) copy-start(bf16[2048,128]{1,0:T(8,128)(2,1)} %param.20) | copy-start | bytes 1572868
  54.4 1.2 copy-start.6
  83.2 117.7 %reduce-scatter.2.cloned.1.call-start = ((), (), s32[]{:S(2)}) async-start(), calls=%async_computation.2 | async-start | bytes 3538944 | tf_op jit(solution)/shard_map/reduce_scatter | solution.py:214
  83.3 3.3 %copy-start.2 = (bf16[768,2048]{1,0:T(8,128)(2,1)S(1)}, bf16[768,2048]{1,0:T(8,128)(2,1)}, u32[]{:S(2)}) copy-start(bf16[768,2048]{1,0:T(8,128)(2,1)} %all-gather.7.cloned.1.call-done) | copy-start | bytes 9437188
  83.3 3.4 %copy-start.7 = (bf16[2048,256]{1,0:T(8,128)(2,1)S(1)}, bf16[2048,256]{1,0:T(8,128)(2,1)}, u32[]{:S(2)}) copy-start(bf16[2048,256]{1,0:T(8,128)(2,1)} %param.27) | copy-start | bytes 3145732
  86.7 3.2 %copy-start.10 = (bf16[2048,128]{1,0:T(8,128)(2,1)S(1)}, bf16[2048,128]{1,0:T(8,128)(2,1)}, u32[]{:S(2)}) copy-start(bf16[2048,128]{1,0:T(8,128)(2,1)} %param.19) | copy-start | bytes 1572868
  87.8 3.1 %copy-start.8 = (bf16[2048,256]{1,0:T(8,128)(2,1)S(1)}, bf16[2048,256]{1,0:T(8,128)(2,1)}, u32[]{:S(2)}) copy-start(bf16[2048,256]{1,0:T(8,128)(2,1)} %param.26) | copy-start | bytes 3145732
  87.8 5.9 %collective-permute-start = (bf16[2,256]{1,0:T(2,128)(2,1)S(1)}, bf16[2,256]{1,0:T(2,128)(2,1)S(1)}, u32[]{:S(2)}, u32[]{:S(2)}) collective-permute-start(bf16[2,256]{1,0:T(2,128)(2,1)S(1)} %slice.392), channel_id=1, source_target_pairs={{0,8},{8,16},{16,24},{24,32},{32,40},{40,48},{48,56},{56,64},{64,7... | collective-permute-start | bytes 3080 | tf_op jit(solution)/shard_map/ppermute | solution.py:21
  145.5 0.7 copy-start.12
  145.5 1.1 copy-start.11
  161.6 1.2 copy-start.3
  161.6 1.3 copy-start.4
Sparse Core Ops, SparseCore 0:
  9.9 33.2 all-gather.6
  83.3 38.0 all-gather.8
  165.9 34.9 reduce-scatter.1
where the time goes:
time: 208 us; the launch traced here: 207 us
  waiting for transfers between devices  94 us (45%)
  between operations  47.3 us (23%)
  blocking collectives  25.9 us (12%)
  matrix products  23.2 us (11%)
  local copies, waits for them, and re-layouts  8.19 us (4%)
  other arithmetic  6.7 us (3%)
  starting transfers between devices  2.14 us (1%)
    reduce_scatter x1, waiting for transfers between devices, per_device(): lax.psum_scatter((jnp.dot(heads_out, w_out_memory, preferred_element_type...  35.1 us
    all_gather x1, waiting for transfers between devices, per_device(): sub_rows = lax.all_gather(normed, 'tp', axis=0, tiled=True)  31.2 us
    all_gather x1, waiting for transfers between devices, collected_together(): both, at, found = (lax.all_gather(jnp.concatenate(lines), axis), 0, {})  27.6 us
    dot_general x8, matrix products, per_device(): jnp.dot(sub_rows, weight, preferred_element_type=jnp.float32)  14.8 us
    all_gather x1, blocking collectives, collected_together(): both, at, found = (lax.all_gather(jnp.concatenate(lines), axis), 0, {})  13.5 us
    psum x1, blocking collectives, per_device(): row_total = lax.psum(local_squares, 'tp')  12.4 us
  transfers between devices with their start and end apart: 4, of which 3 were waited for; matrix products, arithmetic and copies ran while one was open for 5% of the time, Pallas kernels for 0%

commit v1 on v0

--- a/solution.py
+++ b/solution.py
@@ -200,7 +200,11 @@
     denominator = jnp.sum(mixing, axis=2).T + carried * from_norm
     memory_out = numerator / jnp.maximum(jnp.abs(denominator), 1.0)[:, :, None]
     local_squares = jnp.sum(memory_out * memory_out, axis=(1, 2))
-    row_total = lax.psum(local_squares, "tp")
+    row_total = local_squares
+    for hop in (1, 2, 4):
+        row_total = row_total + lax.ppermute(
+            row_total, "tp", [(dev, dev ^ hop) for dev in range(8)]
+        )
     row_scale = lax.rsqrt(row_total / V_WIDTH + epsilon)
     heads_out = memory_out * row_scale[:, None, None]
     heads_out = heads_out.reshape(row_count, value_width).astype(jnp.bfloat16)

time: 208 us -> 210 us (level)
  blocking collectives: 25.9 us -> 13.5 us
  waiting for transfers between devices: 94 us -> 103 us
  starting transfers between devices: 2.14 us -> 8.32 us
    psum x1 -> x0, blocking collectives: 12.4 us -> none  [per_device(): row_total = lax.psum(local_squares, 'tp')]
    ppermute x0 -> x3, starting transfers between devices: none -> 4.85 us  [per_device(): lax.ppermute(row_total, 'tp', [(dev, dev ^ hop) for dev in range(8)])]
    all_gather x1, waiting for transfers between devices: 27.6 us -> 30.8 us  [collected_together(): both, at, found = (lax.all_gather(jnp.concatenate(lines), axis), 0, {})]
    ppermute x0 -> x3, waiting for transfers between devices: none -> 3.15 us  [per_device(): lax.ppermute(row_total, 'tp', [(dev, dev ^ hop) for dev in range(8)])]
  transfers between devices with their start and end apart: 4 -> 7, of which waited for: 3 -> 5; matrix products, arithmetic and copies ran while one was open for 5% -> 4% of each run, Pallas kernels for 0% -> 0%
where the time goes in v1:
time: 210 us
  waiting for transfers between devices  103 us (49%)
  between operations  47.2 us (22%)
  matrix products  22.6 us (11%)
  blocking collectives  13.5 us (6%)
  starting transfers between devices  8.32 us (4%)
  local copies, waits for them, and re-layouts  8.08 us (4%)
  other arithmetic  6.72 us (3%)
    reduce_scatter x1, waiting for transfers between devices, per_device(): lax.psum_scatter((jnp.dot(heads_out, w_out_memory, preferred_element_type...  37 us
    all_gather x1, waiting for transfers between devices, per_device(): sub_rows = lax.all_gather(normed, 'tp', axis=0, tiled=True)  32.1 us
    all_gather x1, waiting for transfers between devices, collected_together(): both, at, found = (lax.all_gather(jnp.concatenate(lines), axis), 0, {})  30.8 us
    dot_general x8, matrix products, per_device(): jnp.dot(sub_rows, weight, preferred_element_type=jnp.float32)  14 us
    all_gather x1, blocking collectives, collected_together(): both, at, found = (lax.all_gather(jnp.concatenate(lines), axis), 0, {})  13.5 us
    ppermute x3, starting transfers between devices, per_device(): lax.ppermute(row_total, 'tp', [(dev, dev ^ hop) for dev in range(8)])  4.85 us
  transfers between devices with their start and end apart: 7, of which 5 were waited for; matrix products, arithmetic and copies ran while one was open for 4% of the time, Pallas kernels for 0%

profile of v1, /device:TPU:2, one launch (start us, length us, event | category | flops | bytes accessed | tf_op | source)
XLA Modules:
  0.0 209.6 jit_solution(14675703359749143935)
XLA Ops:
  6.5 1.3 fusion.4
  7.8 1.9 fusion.6
  9.8 1.2 dynamic_slice.13
  11.0 32.1 %all-gather.7.cloned.1.call-done = bf16[768,2048]{1,0:T(8,128)(2,1)} async-done(((bf16[96,2048]{1,0:T(8,128)(2,1)}), bf16[768,2048]{1,0:T(8,128)(2,1)}) %all-gather.7.cloned.1.call-update) | async-done | bytes 3145744 | tf_op jit(solution)/shard_map/all_gather | solution.py:111
  43.1 2.8 %convolution_reduce_fusion.1 = f32[768]{0:T(1024)S(1)} fusion(bf16[768,2048]{1,0:T(8,128)(2,1)} %all-gather.7.cloned.1.call-done, bf16[2048,8]{0,1:T(8,128)(2,1)} %param.23, s32[]{:T(128)S(6)} %select_n.346), kind=kOutput, calls=%fused_computation.18 | convolution fusion | flops 3145728 | bytes 3156996 | tf_op jit(solution)/shard_map/dot_general | solution.py:113
  46.0 0.6 fusion.118
  46.5 0.3 reduce-window.6
  46.8 0.2 slice_reduce_fusion
  47.0 0.2 reduce-window.9
  47.2 0.6 slice.336
  47.9 0.6 slice.337
  49.6 3.0 %convolution_reduce_fusion = f32[768]{0:T(1024)S(1)} fusion(bf16[768,2048]{1,0:T(8,128)(2,1)} %all-gather.7.cloned.1.call-done, bf16[2048,8]{0,1:T(8,128)(2,1)} %param.22, s32[]{:T(128)S(6)} %select_n.346), kind=kOutput, calls=%fused_computation.17 | convolution fusion | flops 3145728 | bytes 3156996 | tf_op jit(solution)/shard_map/dot_general | solution.py:113
  52.6 0.6 fusion.119
  53.3 0.5 pad.22
  53.8 0.5 subtract_exponential_fusion.1
  54.4 1.0 fusion.19
  55.4 0.2 copy-done.6
  55.6 1.0 convolution_convert_fusion.3
  56.6 0.4 fusion.21
  57.0 13.5 %all-gather.2 = f32[4,131,256]{2,1,0:T(8,128)S(1)} all-gather(f32[1,131,256]{2,1,0:T(8,128)S(1)} %maximum_bitcast_fusion), channel_id=2, replica_groups=mesh['sp_0'=8,'sp_1'=4,'tp'=8] {'sp_1'}, dimensions={0}, use_global_device_ids=true | all-gather | bytes 670720 | tf_op jit(solution)/shard_map/all_gather | solution.py:38
  70.6 0.6 fusion.192
  71.2 0.5 fusion.193
  81.9 0.7 maximum_bitcast_fusion.1
  82.7 0.9 constant_dynamic-slice_fusion
  84.2 3.3 %convolution_convert_fusion = bf16[768,256]{1,0:T(8,128)(2,1)S(1)} fusion(bf16[768,2048]{1,0:T(8,128)(2,1)} %all-gather.7.cloned.1.call-done, bf16[2048,256]{1,0:T(8,128)(2,1)} %param.28), kind=kOutput, calls=%fused_computation.10 | convolution fusion | flops 805502976 | bytes 4587520 | tf_op jit(solution)/shard_map/dot_general | solution.py:113
  87.6 1.0 convolution_convert_fusion.1
  88.7 0.3 select_reduce_fusion
  89.0 1.0 convolution_convert_fusion.5
  90.0 30.8 %all-gather.9.cloned.1.call-done = f32[8,131,256]{2,1,0:T(8,128)} async-done(((f32[1,131,256]{2,1,0:T(8,128)}), f32[8,131,256]{2,1,0:T(8,128)}) %all-gather.9.cloned.1.call-update) | async-done | bytes 1073168 | tf_op jit(solution)/shard_map/all_gather | solution.py:38
  120.8 1.0 fusion.188
  121.8 0.6 fusion.190
  122.4 0.6 fusion.191
  144.7 0.7 fusion.194
  145.5 0.5 convolution_bitcast_fusion
  146.0 0.1 copy-done.12
  146.1 0.5 convolution_reduce_fusion.2
  146.6 2.6 %multiply_reduce_fusion = (f32[768]{0:T(1024)S(1)}, f32[1,256,768]{2,1,0:T(8,128)S(1)}) fusion(f32[768]{0:T(1024)S(1)} %get-tuple-element.5, f32[1,256,768]{2,1,0:T(8,128)S(1)} %convolution_bitcast_fusion, bf16[768,128]{1,0:T(8,128)(2,1)S(1)} %convolution_convert_fusion.5, f32[8,131,256]{2,1,0:T(8,128)} %all-gather.9.cloned.1.call-done, ...), kind=kOutput, calls=%fused_computation.34 | convolution fusion | flops 305200384 | bytes 3902464 | tf_op jit(solution)/shard_map/thd,hdv->thv/dot_general | solution.py:197
  149.4 0.1 multiply_convert_fusion
  149.5 3.4 %collective-permute-start.3 = (bf16[2,256]{1,0:T(2,128)(2,1)S(1)}, bf16[2,256]{1,0:T(2,128)(2,1)S(1)}, u32[]{:S(2)}, u32[]{:S(2)}) collective-permute-start(bf16[2,256]{1,0:T(2,128)(2,1)S(1)} %slice.392), channel_id=1, source_target_pairs={{0,8},{8,16},{16,24},{24,32},{32,40},{40,48},{48,56},{56,64},{64,7... | collective-permute-start | bytes 3080 | tf_op jit(solution)/shard_map/ppermute | solution.py:21
  152.9 1.7 collective-permute-start.1
  154.6 1.0 convolution_convert_fusion.2
  155.6 1.1 collective-permute-done.1
  156.8 3.0 %collective-permute-start.2 = (f32[768]{0:T(1024)S(1)}, f32[768]{0:T(1024)S(1)}, u32[]{:S(2)}, u32[]{:S(2)}) collective-permute-start(f32[768]{0:T(1024)S(1)} %add.433), channel_id=1, source_target_pairs={{0,4},{1,5},{2,6},{3,7},{4,0},{5,1},{6,2},{7,3},{8,12},{9,13},{10,... | collective-permute-start | bytes 9224 | tf_op jit(solution)/shard_map/ppermute | solution.py:205
  159.9 2.0 collective-permute-done.2
  161.9 1.0 fusion.12
  162.9 0.2 copy-done.4
  163.1 2.9 %add_convert_fusion = bf16[768,2048]{1,0:T(8,128)(2,1)} fusion(f32[768,2048]{1,0:T(8,128)S(1)} %fusion.12, bf16[256,2048]{1,0:T(8,128)(2,1)S(1)} %copy-done.4, f32[770,256]{1,0:T(8,128)S(1)} %maximum_convert_fusion, bf16[768,256]{1,0:T(8,128)(2,1)S(1)} %convolution_convert_fusion.2, f32[256]{0:T(256)S(1)} %bitcast.178, f32[256]{0:T(256)S(1)} %bitcast.177, ...), kind=kOutput, calls=%fused_computation | convolution fusion | flops 810024960 | bytes 13241344 | tf_op jit(solution)/shard_map/dot_general | solution.py:221
  166.0 37.0 %reduce-scatter.2.cloned.1.call-done = bf16[96,2048]{1,0:T(8,128)(2,1)} async-done(((bf16[768,2048]{1,0:T(8,128)(2,1)}), bf16[96,2048]{1,0:T(8,128)(2,1)}) %reduce-scatter.2.cloned.1.call-update) | async-done | bytes 393232 | tf_op jit(solution)/shard_map/reduce_scatter | solution.py:218
  (59 shorter events, 0.7 us)
Async XLA Ops:
  6.5 155.4 %copy-start = (bf16[256,2048]{1,0:T(8,128)(2,1)S(1)}, bf16[256,2048]{1,0:T(8,128)(2,1)}, u32[]{:S(2)}) copy-start(bf16[256,2048]{1,0:T(8,128)(2,1)} %param.32) | copy-start | bytes 3145732
  6.5 36.6 %all-gather.7.cloned.1.call-start = ((), (), s32[]{:S(2)}) async-start(), calls=%async_computation.1 | async-start | bytes 3538944 | tf_op jit(solution)/shard_map/all_gather | solution.py:111
  9.8 111.1 %all-gather.9.cloned.1.call-start = ((), (), s32[]{:S(2)}) async-start(), calls=%async_computation.3 | async-start | bytes 1253376 | tf_op jit(solution)/shard_map/all_gather | solution.py:38
  11.0 35.5 %copy-start.5 = (f32[768,1]{0,1:T(1,128)S(1)}, f32[768,1]{0,1:T(1,128)}, u32[]{:S(2)}) copy-start(f32[768,1]{0,1:T(1,128)} %param.25) | copy-start | bytes 9220
  49.6 4.8 %copy-start.1 = (bf16[768,2048]{1,0:T(8,128)(2,1)S(1)}, bf16[768,2048]{1,0:T(8,128)(2,1)}, u32[]{:S(2)}) copy-start(bf16[768,2048]{1,0:T(8,128)(2,1)} %all-gather.7.cloned.1.call-done) | copy-start | bytes 9437188
  49.6 4.8 %copy-start.9 = (bf16[2048,128]{1,0:T(8,128)(2,1)S(1)}, bf16[2048,128]{1,0:T(8,128)(2,1)}, u32[]{:S(2)}) copy-start(bf16[2048,128]{1,0:T(8,128)(2,1)} %param.20) | copy-start | bytes 1572868
  54.4 1.2 copy-start.6
  82.6 120.4 %reduce-scatter.2.cloned.1.call-start = ((), (), s32[]{:S(2)}) async-start(), calls=%async_computation.2 | async-start | bytes 3538944 | tf_op jit(solution)/shard_map/reduce_scatter | solution.py:218
  84.1 3.3 %copy-start.2 = (bf16[768,2048]{1,0:T(8,128)(2,1)S(1)}, bf16[768,2048]{1,0:T(8,128)(2,1)}, u32[]{:S(2)}) copy-start(bf16[768,2048]{1,0:T(8,128)(2,1)} %all-gather.7.cloned.1.call-done) | copy-start | bytes 9437188
  84.1 3.4 %copy-start.7 = (bf16[2048,256]{1,0:T(8,128)(2,1)S(1)}, bf16[2048,256]{1,0:T(8,128)(2,1)}, u32[]{:S(2)}) copy-start(bf16[2048,256]{1,0:T(8,128)(2,1)} %param.27) | copy-start | bytes 3145732
  87.6 1.4 copy-start.10
  145.4 0.7 copy-start.12
  145.4 1.1 copy-start.11
  146.6 8.0 %copy-start.3 = (bf16[768,2048]{1,0:T(8,128)(2,1)S(1)}, bf16[768,2048]{1,0:T(8,128)(2,1)}, u32[]{:S(2)}) copy-start(bf16[768,2048]{1,0:T(8,128)(2,1)} %all-gather.7.cloned.1.call-done) | copy-start | bytes 9437188
  146.6 8.0 %copy-start.8 = (bf16[2048,256]{1,0:T(8,128)(2,1)S(1)}, bf16[2048,256]{1,0:T(8,128)(2,1)}, u32[]{:S(2)}) copy-start(bf16[2048,256]{1,0:T(8,128)(2,1)} %param.26) | copy-start | bytes 3145732
  149.3 3.6 %collective-permute-start = (f32[768]{0:T(1024)S(1)}, f32[768]{0:T(1024)S(1)}, u32[]{:S(2)}, u32[]{:S(2)}) collective-permute-start(f32[768]{0:T(1024)S(1)} %get-tuple-element.48), channel_id=1, source_target_pairs={{0,1},{1,0},{2,3},{3,2},{4,5},{5,4},{6,7},{7,6},{8,9},{9,8},{10,11... | collective-permute-start | bytes 9224 | tf_op jit(solution)/shard_map/ppermute | solution.py:205
  149.5 10.3 %collective-permute-start.3 = (bf16[2,256]{1,0:T(2,128)(2,1)S(1)}, bf16[2,256]{1,0:T(2,128)(2,1)S(1)}, u32[]{:S(2)}, u32[]{:S(2)}) collective-permute-start(bf16[2,256]{1,0:T(2,128)(2,1)S(1)} %slice.392), channel_id=1, source_target_pairs={{0,8},{8,16},{16,24},{24,32},{32,40},{40,48},{48,56},{56,64},{64,7... | collective-permute-start | bytes 3080 | tf_op jit(solution)/shard_map/ppermute | solution.py:21
  152.9 3.9 %collective-permute-start.1 = (f32[768]{0:T(1024)S(1)}, f32[768]{0:T(1024)S(1)}, u32[]{:S(2)}, u32[]{:S(2)}) collective-permute-start(f32[768]{0:T(1024)S(1)} %add.432), channel_id=1, source_target_pairs={{0,2},{1,3},{2,0},{3,1},{4,6},{5,7},{6,4},{7,5},{8,10},{9,11},{10,... | collective-permute-start | bytes 9224 | tf_op jit(solution)/shard_map/ppermute | solution.py:205
  156.8 5.1 %collective-permute-start.2 = (f32[768]{0:T(1024)S(1)}, f32[768]{0:T(1024)S(1)}, u32[]{:S(2)}, u32[]{:S(2)}) collective-permute-start(f32[768]{0:T(1024)S(1)} %add.433), channel_id=1, source_target_pairs={{0,4},{1,5},{2,6},{3,7},{4,0},{5,1},{6,2},{7,3},{8,12},{9,13},{10,... | collective-permute-start | bytes 9224 | tf_op jit(solution)/shard_map/ppermute | solution.py:205
  161.9 1.2 copy-start.4
Sparse Core Ops, SparseCore 0:
  9.9 33.2 all-gather.6
  82.7 38.0 all-gather.8
  166.2 36.8 reduce-scatter.1
